TPU v7x, 128 devices: a whole 4x4x4 slice. The times are simulated.
128 devices in a mesh: rep: 2 (over z_hi), fs: 32 (over z_lo, y, x), tp: 2 (over core).
Axes of the slice: x: 4, y: 4, z: 4 (z_hi: 2, z_lo: 2; z = z_hi * 2 + z_lo), core: 2. Of those that a mesh axis runs over, the one named last changes fastest.
Arguments:
- tokens: bfloat16 [65536, 2048], P(('rep', 'fs')), may hold values from -6 to 6
- norm_mix: bfloat16 [2048], replicated, may hold values from 0.099609375 to 1.8984375
- w_unit: bfloat16 [2048, 1024], P('fs', 'tp'), may hold values from -0.125 to 0.125
- w_value: bfloat16 [2048, 1024], P('fs', 'tp'), may hold values from -0.125 to 0.125
- spatial: bfloat16 [4, 128, 128], replicated, may hold values from -0.52734375 to 0.52734375
- spatial_bias: bfloat16 [4, 128], replicated, may hold values from 0.099609375 to 1.8984375
- group_gain: bfloat16 [1024], replicated, may hold values from 0.099609375 to 1.8984375
- group_shift: bfloat16 [1024], replicated, may hold values from -3 to 3
- w_mix_out: bfloat16 [1024, 2048], P('tp', 'fs'), may hold values from -0.1875 to 0.1875
- norm_ffn: bfloat16 [2048], replicated, may hold values from 0.099609375 to 1.8984375
- w_gate: bfloat16 [2048, 2816], P('fs', 'tp'), may hold values from -0.125 to 0.125
- w_up: bfloat16 [2048, 2816], P('fs', 'tp'), may hold values from -0.125 to 0.125
- w_down: bfloat16 [2816, 2048], P('tp', 'fs'), may hold values from -0.109375 to 0.109375
Outputs:
- layer_out: bfloat16 [65536, 2048], P(('rep', 'fs', 'tp'))
All inputs are finite; a program needn't handle non-finite values.
Results may differ from a plain program's by a relative error of at most 0.008.
Values may be sent and summed in bfloat16 or wider, within the bound.
A program may use at most 128 MiB of HBM per device.

v0:
```python
import jax
import jax.numpy as jnp
from jax import lax
from jax.sharding import PartitionSpec as P


def sent_together(arrays, axis, dim, along):
    ends, at = ([], 0)
    for a in arrays[:-1]:
        at += a.shape[along]
        ends.append(at)
    both = jnp.concatenate(arrays, axis=along)
    return tuple(jnp.split(lax.all_gather(both, axis, axis=dim, tiled=True), ends, axis=along))


def sent_to_all(x, axis):
    copies = jnp.broadcast_to(x, (lax.axis_size(axis), *x.shape))
    return lax.all_to_all(copies, axis, split_axis=0, concat_axis=0, tiled=True)


def in_order(pieces, dim):
    pieces = jnp.moveaxis(pieces, 0, dim)
    dims = pieces.shape
    return pieces.reshape(*dims[:dim], dims[dim] * dims[dim + 1], *dims[dim + 2 :])


def gathered_copies(x, axis, dim):
    pieces = sent_to_all(x, axis)
    return in_order(pieces, dim)


def total_of_pieces(x, axis):
    return lax.all_gather(x, axis).sum(0)


def split_up(x, dim, peers):
    before, after = (x.shape[:dim], x.shape[dim + 1 :])
    return jnp.moveaxis(x.reshape(*before, peers, -1, *after), dim, 0)


def summed_on_arrival(x, axis, dim):
    pieces = split_up(x, dim, lax.axis_size(axis))
    arrived = lax.all_to_all(pieces, axis, split_axis=0, concat_axis=0, tiled=True)
    return arrived.astype(jnp.float32).sum(axis=0)


def rms_scale(values, gain):
    values = values.astype(jnp.float32)
    scale = lax.rsqrt(jnp.mean(values * values, axis=-1, keepdims=True) + 1e-06)
    return values * scale * gain.astype(jnp.float32)


def spatial_unit(unit_pre, value_pre, spatial, spatial_bias, group_gain, group_shift):
    count, width = value_pre.shape
    groups = spatial.shape[0]
    block = spatial.shape[1]
    active = jax.nn.gelu(value_pre, approximate=True).reshape(count, groups, width // groups)
    center = jnp.mean(active, axis=-1, keepdims=True)
    spread = jnp.mean(jnp.square(active - center), axis=-1, keepdims=True)
    normal = ((active - center) * lax.rsqrt(spread + 1e-06)).reshape(count, width)
    normal = normal * group_gain.astype(jnp.float32) + group_shift.astype(jnp.float32)
    grouped = normal.astype(jnp.bfloat16)
    causal = jnp.tril(jnp.ones((block, block), dtype=bool))
    weights = jnp.where(causal[None], spatial, jnp.zeros_like(spatial))
    tiles = grouped.reshape(count // block, block, groups, width // groups)
    mixed = jnp.einsum("gts,nsgd->ntgd", weights, tiles, preferred_element_type=jnp.float32)
    mixed = mixed + spatial_bias.astype(jnp.float32).T[None, :, :, None]
    return jax.nn.gelu(unit_pre, approximate=True) * mixed.reshape(count, width)


def on_device(
    tokens,
    norm_mix,
    w_unit,
    w_value,
    spatial,
    spatial_bias,
    group_gain,
    group_shift,
    w_mix_out,
    norm_ffn,
    w_gate,
    w_up,
    w_down,
):
    count = tokens.shape[0]
    half = count // lax.axis_size("tp")
    position = lax.axis_index("tp")
    row_start = position * half
    local_width = w_unit.shape[1]
    group_count = spatial.shape[0] // lax.axis_size("tp")
    group_start = position * group_count
    spatial_local = lax.dynamic_slice_in_dim(spatial, group_start, group_count, 0)
    bias_local = lax.dynamic_slice_in_dim(spatial_bias, group_start, group_count, 0)
    gain_local = lax.dynamic_slice_in_dim(group_gain, position * local_width, local_width, 0)
    shift_local = lax.dynamic_slice_in_dim(group_shift, position * local_width, local_width, 0)
    normed = rms_scale(tokens, norm_mix).astype(jnp.bfloat16)
    unit_whole, value_whole = sent_together((w_unit, w_value), "fs", 0, 1)
    unit_pre = jnp.dot(normed, unit_whole, preferred_element_type=jnp.float32)
    value_pre = jnp.dot(normed, value_whole, preferred_element_type=jnp.float32)
    gated = spatial_unit(
        unit_pre, value_pre, spatial_local, bias_local, gain_local, shift_local
    ).astype(jnp.bfloat16)
    partial_terms = jnp.dot(
        gated, gathered_copies(w_mix_out, "fs", 1), preferred_element_type=jnp.float32
    )
    summed = total_of_pieces(partial_terms, "tp")
    h_mid = (tokens.astype(jnp.float32) + summed).astype(jnp.bfloat16)
    normed_mid = rms_scale(h_mid, norm_ffn).astype(jnp.bfloat16)
    gate_whole, up_whole = sent_together((w_gate, w_up), "fs", 0, 1)
    gate = jnp.dot(normed_mid, gate_whole, preferred_element_type=jnp.float32)
    up = jnp.dot(normed_mid, up_whole, preferred_element_type=jnp.float32)
    hidden = (jax.nn.silu(gate) * up).astype(jnp.bfloat16)
    down_cols = lax.all_gather(w_down, "fs", axis=1, tiled=True)
    residual_rows = lax.dynamic_slice_in_dim(h_mid, row_start, half, 0).astype(jnp.float32)
    summed_rows = summed_on_arrival(
        jnp.dot(hidden, down_cols, preferred_element_type=jnp.float32).astype(jnp.bfloat16), "tp", 0
    )
    return (residual_rows + summed_rows).astype(jnp.bfloat16)


def solution(mesh):
    placed = (
        P(("rep", "fs"), None),
        P(),
        P("fs", "tp"),
        P("fs", "tp"),
        P(),
        P(),
        P(),
        P(),
        P("tp", "fs"),
        P(),
        P("fs", "tp"),
        P("fs", "tp"),
        P("tp", "fs"),
    )
    return jax.shard_map(
        on_device,
        mesh=mesh,
        in_specs=placed,
        out_specs=P(("rep", "fs", "tp"), None),
        check_vma=False,
    )
```

profile of v0, /device:TPU:1, one launch (start us, length us, event | category | flops | bytes accessed | tf_op | source)
XLA Modules:
  0.0 629.2 jit_solution(16438548954573870074)
XLA Ops:
  6.6 1.6 pad_maximum_fusion.1
  8.2 2.4 broadcast_in_dim.13
  10.6 9.3 %all-to-all-start = ((bf16[32,512,64]{1,2,0:T(8,128)(2,1)}), bf16[32,512,64]{1,2,0:T(8,128)(2,1)}, u32[]{:S(2)}, u32[]{:S(2)}) async-start(bf16[32,512,64]{1,2,0:T(8,128)(2,1)} %broadcast_in_dim.13), calls=%async_computation | async-start | bytes 4194304 | tf_op jit(solution)/shard_map/all_to_all | solution.py:18
  20.1 3.1 fusion.3
  23.3 133.9 %all-gather.6.cloned.1.call-done = bf16[2048,1024]{1,0:T(8,128)(2,1)} async-done(((bf16[64,1024]{1,0:T(8,128)(2,1)}), bf16[2048,1024]{1,0:T(8,128)(2,1)}) %all-gather.6.cloned.1.call-update) | async-done | bytes 4194320 | tf_op jit(solution)/shard_map/all_gather | solution.py:13
  157.1 6.9 %fusion.35 = f32[1024,512]{1,0:T(8,128)} fusion(bf16[2048,1024]{1,0:T(8,128)(2,1)} %all-gather.6.cloned.1.call-done, bf16[1024,2048]{1,0:T(8,128)(2,1)} %param.13, f32[2048]{0:T(1024)S(1)} %convert_element_type.51, f32[1024]{0:T(1024)S(1)} %add_rsqrt_fusion.2), kind=kOutput, calls=%fused_computation.39 | convolution fusion | flops 2160066560 | bytes 8400896 | tf_op jit(solution)/shard_map/dot_general | solution.py:100
  164.1 2.6 reshape.58
  166.7 1.2 reduce_sum.55
  167.9 14.4 %multiply_reduce_fusion = f32[1024,2]{1,0:T(8,128)S(1)} fusion(f32[1024,2,256]{2,1,0:T(2,128)S(1)} %reshape.58, f32[1024,2]{1,0:T(8,128)S(1)} %broadcast_multiply_fusion), kind=kLoop, calls=%fused_computation.46 | loop fusion | flops 1570816 | bytes 2113536 | tf_op jit(solution)/shard_map/reduce_sum | solution.py:59
  182.4 1.2 mul.112
  183.8 1.2 sub.17
  187.1 2.4 copy.28
  189.5 1.8 copy.33
  191.3 11.6 %fusion.51 = f32[1024,2048]{1,0:T(8,128)} fusion(bf16[512,2048]{0,1:T(8,128)(2,1)} %bitcast.5, f32[1024,512]{1,0:T(8,128)S(1)} %bitcast.30, bf16[2048,1024]{1,0:T(8,128)(2,1)} %all-gather.6.cloned.1.call-done, bf16[1024,2048]{1,0:T(8,128)(2,1)} %param.13, f32[2048]{0:T(1024)S(1)} %convert_element_type.51, f32[1024]{0:T(1024)S(1)} %add_rsqrt_fusion.2), kind=kOutput, calls=%fused_computation.47 | convolution fusion | flops 4308598784 | bytes 18886656 | tf_op jit(solution)/shard_map/dot_general | solution.py:104
  205.3 49.1 %all-gather.12.cloned.1.call-done = f32[2048,2048]{1,0:T(8,128)} async-done(((f32[1024,2048]{1,0:T(8,128)}), f32[2048,2048]{1,0:T(8,128)}) %all-gather.12.cloned.1.call-update) | async-done | bytes 16777232 | tf_op jit(solution)/shard_map/all_gather | solution.py:33
  254.4 11.8 %reduce_sum.57 = f32[1024,2048]{1,0:T(8,128)} reduce(f32[2,1024,2048]{2,1,0:T(8,128)} %bitcast.23, f32[]{:T(128)} %constant.15.clone.1), dimensions={0}, to_apply=%region_3.4 | reduce | flops 2097152 | bytes 25165828 | tf_op jit(solution)/shard_map/reduce_sum | solution.py:33
  266.1 7.8 %fusion = (f32[1024]{0:T(1024)S(1)}, bf16[1024,2048]{1,0:T(8,128)(2,1)}) fusion(f32[1024,2048]{1,0:T(8,128)} %reduce_sum.57, bf16[1024,2048]{1,0:T(8,128)(2,1)} %param.13), kind=kLoop, calls=%fused_computation.5 | loop fusion | flops 12581888 | bytes 16781312 | tf_op jit(solution)/shard_map/reduce_sum | solution.py:49
  273.9 135.7 %all-gather.8.cloned.1.call-done = bf16[2048,2816]{1,0:T(8,128)(2,1)} async-done(((bf16[64,2816]{1,0:T(8,128)(2,1)}), bf16[2048,2816]{1,0:T(8,128)(2,1)}) %all-gather.8.cloned.1.call-update) | async-done | bytes 11534352 | tf_op jit(solution)/shard_map/all_gather | solution.py:13
  409.6 11.9 %fusion.9 = f32[1024,1408]{1,0:T(8,128)} fusion(bf16[2048,2816]{1,0:T(8,128)(2,1)} %all-gather.8.cloned.1.call-done, bf16[1024,2048]{1,0:T(8,128)(2,1)} %get-tuple-element.6, f32[2048]{0:T(1024)S(1)} %convert_element_type.60, f32[1024]{0:T(1024)S(1)} %add_rsqrt_fusion.1), kind=kOutput, calls=%fused_computation.15 | convolution fusion | flops 5913968640 | bytes 15740928 | tf_op jit(solution)/shard_map/dot_general | solution.py:111
  421.5 147.9 %all-gather.10.cloned.1.call-done = bf16[1408,2048]{0,1:T(8,128)(2,1)} async-done(((bf16[1408,64]{0,1:T(8,128)(2,1)}), bf16[1408,2048]{0,1:T(8,128)(2,1)}) %all-gather.10.cloned.1.call-update) | async-done | bytes 5767184 | tf_op jit(solution)/shard_map/all_gather | solution.py:114
  569.4 20.9 %fusion.16 = bf16[1024,2048]{1,0:T(8,128)(2,1)} fusion(bf16[1408,2048]{0,1:T(8,128)(2,1)} %all-gather.10.cloned.1.call-done, f32[1024,1408]{1,0:T(8,128)} %fusion.9, bf16[2048,2816]{1,0:T(8,128)(2,1)} %all-gather.8.cloned.1.call-done, bf16[1024,2048]{1,0:T(8,128)(2,1)} %get-tuple-element.6, f32[2048]{0:T(1024)S(1)} %convert_element_type.60, ...), kind=kOutput, calls=%fused_computation.20 | convolution fusion | flops 11830296576 | bytes 25702400 | tf_op jit(solution)/shard_map/dot_general | solution.py:117
  590.3 28.2 %all_to_all.10 = bf16[2,512,2048]{2,1,0:T(8,128)(2,1)S(1)} all-to-all(bf16[2,512,2048]{2,1,0:T(8,128)(2,1)} %bitcast.29), channel_id=1, replica_groups=mesh['rep'=2,'fs'=32,'tp'=2] {'tp'}, dimensions={0} | all-to-all | bytes 8388608 | tf_op jit(solution)/shard_map/all_to_all | solution.py:43
  619.4 1.2 copy-done
  620.7 2.1 add_convert_fusion
  (44 shorter events, 5.8 us)
Async XLA Ops:
  6.5 13.4 %copy-start.5 = (bf16[2048]{0:T(1024)(128)(2,1)S(1)}, bf16[2048]{0:T(1024)(128)(2,1)}, u32[]{:S(2)}) copy-start(bf16[2048]{0:T(1024)(128)(2,1)} %param.14) | copy-start | bytes 12292
  6.5 13.5 %copy-start.9 = (bf16[4,128]{1,0:T(4,128)(2,1)S(1)}, bf16[4,128]{1,0:T(4,128)(2,1)}, u32[]{:S(2)}) copy-start(bf16[4,128]{1,0:T(4,128)(2,1)} %param.18) | copy-start | bytes 3076
  6.5 13.5 %copy-start.8 = (bf16[1024]{0:T(1024)(128)(2,1)S(1)}, bf16[1024]{0:T(1024)(128)(2,1)}, u32[]{:S(2)}) copy-start(bf16[1024]{0:T(1024)(128)(2,1)} %param.19) | copy-start | bytes 6148
  6.5 13.5 %copy-start.7 = (bf16[1024]{0:T(1024)(128)(2,1)S(1)}, bf16[1024]{0:T(1024)(128)(2,1)}, u32[]{:S(2)}) copy-start(bf16[1024]{0:T(1024)(128)(2,1)} %param.20) | copy-start | bytes 6148
  6.5 150.6 %all-gather.6.cloned.1.call-start = ((), (), s32[]{:S(2)}) async-start(), calls=%async_computation.2 | async-start | bytes 4325376 | tf_op jit(solution)/shard_map/all_gather | solution.py:13
  10.6 180.7 %all-to-all-start = ((bf16[32,512,64]{1,2,0:T(8,128)(2,1)}), bf16[32,512,64]{1,2,0:T(8,128)(2,1)}, u32[]{:S(2)}, u32[]{:S(2)}) async-start(bf16[32,512,64]{1,2,0:T(8,128)(2,1)} %broadcast_in_dim.13), calls=%async_computation | async-start | bytes 4194304 | tf_op jit(solution)/shard_map/all_to_all | solution.py:18
  19.9 234.4 %all-gather.12.cloned.1.call-start = ((), (), s32[]{:S(2)}) async-start(), calls=%async_computation.5 | async-start | bytes 25165824 | tf_op jit(solution)/shard_map/all_gather | solution.py:33
  183.8 1.6 copy-start.1
  185.4 1.1 copy-start.4
  202.9 0.9 copy-start.2
  202.9 1.0 copy-start.3
  202.9 2.4 copy-start.6
  202.9 206.7 %all-gather.8.cloned.1.call-start = ((), (), s32[]{:S(2)}) async-start(), calls=%async_computation.3 | async-start | bytes 11894784 | tf_op jit(solution)/shard_map/all_gather | solution.py:13
  204.7 364.7 %all-gather.10.cloned.1.call-start = ((), (), s32[]{:S(2)}) async-start(), calls=%async_computation.4 | async-start | bytes 5947392 | tf_op jit(solution)/shard_map/all_gather | solution.py:114
  618.5 2.2 copy-start
Sparse Core Ops, SparseCore 0:
  9.0 148.1 all-gather.5
  203.0 51.2 all-gather.11
  256.0 153.5 all-gather.7
  411.1 158.2 all-gather.9
where the time goes:
time: 630 us; the launch traced here: 629 us
  waiting for transfers between devices  467 us (74%)
  matrix products  51.8 us (8%)
  other arithmetic  44.6 us (7%)
  blocking collectives  28.2 us (4%)
  local copies, waits for them, and re-layouts  14.5 us (2%)
  between operations  13.3 us (2%)
  starting transfers between devices  9.5 us (2%)
    all_gather x2, waiting for transfers between devices, sent_together(): lax.all_gather(both, axis, axis=dim, tiled=True)  270 us
    all_gather x1, waiting for transfers between devices, on_device(): down_cols = lax.all_gather(w_down, 'fs', axis=1, tiled=True)  148 us
    all_gather x1, waiting for transfers between devices, total_of_pieces(): return lax.all_gather(x, axis).sum(0)  49.1 us
    all_to_all x1, blocking collectives, summed_on_arrival(): lax.all_to_all(pieces, axis, split_axis=0, concat_axis=0, tiled=True)  28.2 us
    dot_general x1, matrix products, on_device(): jnp.dot(hidden, down_cols, preferred_element_type=jnp.float32)  20.9 us
    reduce_sum x1, other arithmetic, spatial_unit(): spread = jnp.mean(jnp.square(active - center), axis=-1, keepdims=True)  14.4 us
  transfers between devices with their start and end apart: 5, of which 4 were waited for; matrix products, arithmetic and copies ran while one was open for 11% of the time, Pallas kernels for 0%

commit v1 on v0

v1 whole, which is shorter than its diff:
```python
import functools

import jax
import jax.numpy as jnp
from jax import lax
from jax.experimental import pallas as pl
from jax.experimental.pallas import tpu as pltpu
from jax.sharding import PartitionSpec as P

MESH = pl.DeviceIdType.MESH
F32 = jnp.float32
BF16 = jnp.bfloat16
LANES = 128

UNIT, VALUE, MIX, PAIRS, DOWN = 0, 512, 1024, 1536, 4352
WIDTH = 5760
HALF_FF = 1408

FLOWS = (
    (0, 5, 0),
    (5, 3, 1),
    (8, 3, 0),
    (11, 1, 1),
    (12, 5, 0),
    (17, 3, 1),
    (20, 5, 0),
    (25, 3, 1),
    (28, 4, 0),
    (32, 2, 1),
    (34, 4, 0),
    (38, 2, 1),
    (40, 3, 0),
    (43, 2, 1),
)
SENDS = 14


class Flow:
    def __init__(self, index, buf, send_sems, recv_sems, where):
        first, tiles, self.order = FLOWS[index]
        self.index = index
        self.cols = pl.ds(first * LANES, tiles * LANES)
        self.buf, self.send_sems, self.recv_sems = buf, send_sems, recv_sems
        self.where = where
        self.sent = []

    def part(self, t, z, y, x, rows):
        row = {0: pl.ds(0, 64), 1: pl.ds(0, 32), 2: pl.ds(32, 32)}[rows]
        every = slice(None)
        pick = lambda i: every if i is None else i
        return self.buf.at[t, pick(z), pick(y), pick(x), row, self.cols]

    def copy(self, slot, ref, device):
        return pltpu.make_async_remote_copy(
            src_ref=ref,
            dst_ref=ref,
            send_sem=self.send_sems.at[self.index, slot],
            recv_sem=self.recv_sems.at[self.index, slot],
            device_id=device,
            device_id_type=MESH,
        )

    def send(self, slot, ref, device):
        copy = self.copy(slot, ref, device)
        copy.start()
        self.sent.append(copy)

    def arrived(self, slot, ref, device):
        self.copy(slot, ref, device).wait_recv()

    def stage(self, number):
        (self.order_xyz if self.order == 0 else self.order_zyx)(number)

    def order_xyz(self, number):
        t, z, y, x, to = self.where
        part = lambda dz, dy, dx, rows: self.part(
            t,
            lax.rem(z + dz, 2),
            None if dy is None else lax.rem(y + dy, 4),
            None if dx is None else lax.rem(x + dx, 4),
            rows,
        )
        if number == 0:
            own = part(0, 0, 0, 0)
            self.send(0, own, to["x+"])
            self.send(1, own, to["x-"])
        elif number == 1:
            self.arrived(0, part(0, 0, 3, 0), to["x-"])
            self.send(2, part(0, 0, 3, 1), to["x+"])
            self.arrived(1, part(0, 0, 1, 0), to["x+"])
            self.send(3, part(0, 0, 1, 2), to["x-"])
        elif number == 2:
            self.arrived(2, part(0, 0, 2, 1), to["x-"])
            self.arrived(3, part(0, 0, 2, 2), to["x+"])
            row = part(0, 0, None, 0)
            self.send(4, row, to["y+"])
            self.send(5, row, to["y-"])
        elif number == 3:
            self.arrived(4, part(0, 3, None, 0), to["y-"])
            self.send(6, part(0, 3, None, 1), to["y+"])
            self.arrived(5, part(0, 1, None, 0), to["y+"])
            self.send(7, part(0, 1, None, 2), to["y-"])
        elif number == 4:
            self.arrived(6, part(0, 2, None, 1), to["y-"])
            self.arrived(7, part(0, 2, None, 2), to["y+"])
            self.send(8, part(0, None, None, 1), to["z+"])
            self.send(9, part(0, None, None, 2), to["z-"])
            self.send(10, part(0, None, None, 0), to["core"])
        elif number == 5:
            self.arrived(8, part(1, None, None, 1), to["z-"])
            self.arrived(9, part(1, None, None, 2), to["z+"])
            self.send(11, part(1, None, None, 0), to["core"])
        else:
            other = 1 - t
            self.arrived(10, self.part(other, z, None, None, 0), to["core"])
            self.arrived(11, self.part(other, 1 - z, None, None, 0), to["core"])

    def order_zyx(self, number):
        t, z, y, x, to = self.where
        part = lambda dz, dy, dx, rows: self.part(
            t,
            None if dz is None else lax.rem(z + dz, 2),
            None if dy is None else lax.rem(y + dy, 4),
            lax.rem(x + dx, 4),
            rows,
        )
        if number == 0:
            self.send(0, part(0, 0, 0, 1), to["z+"])
            self.send(1, part(0, 0, 0, 2), to["z-"])
        elif number == 1:
            self.arrived(0, part(1, 0, 0, 1), to["z-"])
            self.arrived(1, part(1, 0, 0, 2), to["z+"])
            pair = part(None, 0, 0, 0)
            self.send(2, pair, to["y+"])
            self.send(3, pair, to["y-"])
        elif number == 2:
            self.arrived(2, part(None, 3, 0, 0), to["y-"])
            self.send(4, part(None, 3, 0, 1), to["y+"])
            self.arrived(3, part(None, 1, 0, 0), to["y+"])
            self.send(5, part(None, 1, 0, 2), to["y-"])
        elif number == 3:
            self.arrived(4, part(None, 2, 0, 1), to["y-"])
            self.arrived(5, part(None, 2, 0, 2), to["y+"])
            line = part(None, None, 0, 0)
            self.send(6, line, to["x+"])
            self.send(7, line, to["x-"])
            self.send(10, line, to["core"])
        elif number == 4:
            self.arrived(6, part(None, None, 3, 0), to["x-"])
            self.send(8, part(None, None, 3, 1), to["x+"])
            self.arrived(7, part(None, None, 1, 0), to["x+"])
            self.send(9, part(None, None, 1, 2), to["x-"])
            self.send(11, part(None, None, 3, 0), to["core"])
            self.send(12, part(None, None, 1, 0), to["core"])
        elif number == 5:
            self.arrived(8, part(None, None, 2, 1), to["x-"])
            self.arrived(9, part(None, None, 2, 2), to["x+"])
            self.send(13, part(None, None, 2, 0), to["core"])
        else:
            other = 1 - t
            for slot, dx in ((10, 0), (11, 3), (12, 1), (13, 2)):
                place = lax.rem(x + dx, 4)
                self.arrived(slot, self.part(other, None, None, place, 0), to["core"])


def rms_rows(source, gain, target, rows):
    values = source[rows, :].astype(F32)
    scale = lax.rsqrt(jnp.mean(values * values, axis=-1, keepdims=True) + 1e-06)
    target[rows, :] = (values * scale * gain[...].astype(F32)).astype(BF16)


def dot(a, b):
    return jnp.dot(a, b, preferred_element_type=F32)


def dot_nt(a, b):
    return lax.dot_general(a, b, (((1,), (1,)), ((), ())), preferred_element_type=F32)


def kernel(
    tokens,
    shard,
    norm_mix,
    spatial,
    bias,
    gain,
    shift,
    norm_ffn,
    out,
    buf,
    rows_in,
    normed,
    pre,
    gated,
    hmid,
    hidden,
    staged,
    send_sems,
    recv_sems,
    local_sems,
    out_sems,
):
    r, f, t = lax.axis_index("rep"), lax.axis_index("fs"), lax.axis_index("tp")
    z, y, x = f // 16, lax.rem(f // 4, 4), lax.rem(f, 4)
    up, down = lax.rem(2 * r + z + 1, 4), lax.rem(2 * r + z + 3, 4)
    at = lambda zz, yy, xx, tt: (zz // 2, lax.rem(zz, 2) * 16 + yy * 4 + xx, tt)
    here = 2 * r + z
    to = {
        "x+": at(here, y, lax.rem(x + 1, 4), t),
        "x-": at(here, y, lax.rem(x + 3, 4), t),
        "y+": at(here, lax.rem(y + 1, 4), x, t),
        "y-": at(here, lax.rem(y + 3, 4), x, t),
        "z+": at(up, y, x, t),
        "z-": at(down, y, x, t),
        "core": at(here, y, x, 1 - t),
    }

    own = pltpu.make_async_copy(shard, buf.at[t, z, y, x], local_sems.at[0])
    own.start()
    count = rows_in.shape[0]
    load = pltpu.make_async_copy(
        tokens.at[pl.ds(t * count, count)], rows_in, local_sems.at[1]
    )
    load.start()

    barrier = pltpu.get_barrier_semaphore()
    for device in to.values():
        pl.semaphore_signal(barrier, inc=1, device_id=device, device_id_type=MESH)
    pl.semaphore_wait(barrier, len(to))
    own.wait()

    where = (t, z, y, x, to)
    flows = [Flow(i, buf, send_sems, recv_sems, where) for i in range(len(FLOWS))]
    for flow in flows:
        flow.stage(0)
    load.wait()

    blocks = count // LANES

    def over_rows(body):
        def step(i, carry):
            body(pl.ds(pl.multiple_of(i * LANES, LANES), LANES))
            return carry

        lax.fori_loop(0, blocks, step, 0)

    def columns(tt, first, size):
        return buf[tt, :, :, :, :, pl.ds(first, size)].reshape(2048, size)

    def spatial_group(g):
        tt, low = g // 2, (g % 2) * 256
        pre[:, 0:256] = dot(normed[...], columns(tt, UNIT + low, 256))
        pre[:, 256:512] = dot(normed[...], columns(tt, VALUE + low, 256))
        at_row = lax.broadcasted_iota(jnp.int32, (128, 128), 0)
        at_col = lax.broadcasted_iota(jnp.int32, (128, 128), 1)
        weights = jnp.where(at_row >= at_col, spatial[g], jnp.zeros((128, 128), BF16))
        g_gain = gain[:, g * 256 : g * 256 + 256].astype(F32)
        g_shift = shift[:, g * 256 : g * 256 + 256].astype(F32)

        def body(rows):
            active = jax.nn.gelu(pre[rows, 256:512], approximate=True)
            center = jnp.mean(active, axis=-1, keepdims=True)
            off = active - center
            spread = jnp.mean(off * off, axis=-1, keepdims=True)
            grouped = off * lax.rsqrt(spread + 1e-06) * g_gain + g_shift
            mixed = dot(weights, grouped.astype(BF16)) + bias[g]
            value = jax.nn.gelu(pre[rows, 0:256], approximate=True) * mixed
            gated[rows, g * 256 : g * 256 + 256] = value.astype(BF16)

        over_rows(body)

    def mix_out(block, carry):
        zz, yy = block // 4, lax.rem(block, 4)
        cols = pl.ds(pl.multiple_of(block * 256, 256), 256)
        total = rows_in[:, cols].astype(F32)
        for tt in range(2):
            w = buf[tt, zz, yy, :, :, pl.ds(MIX, 512)].reshape(256, 512)
            total = total + dot_nt(gated[:, tt * 512 : tt * 512 + 512], w)
        hmid[:, cols] = total.astype(BF16)
        return carry

    def gate_up(tt):
        def step(i, carry):
            first = pl.multiple_of(PAIRS + i * 256, 256)
            both = dot(normed[...], columns(tt, first, 256))
            value = jax.nn.silu(both[:, 0:128]) * both[:, 128:256]
            into = pl.ds(pl.multiple_of(tt * HALF_FF + i * 128, 128), 128)
            hidden[:, into] = value.astype(BF16)
            return carry

        return step

    def out_copy(block, slot):
        cols = pl.ds(pl.multiple_of(block * 256, 256), 256)
        return pltpu.make_async_copy(
            staged.at[slot], out.at[:, cols], out_sems.at[slot]
        )

    def project_down(block, carry):
        zz, yy = block // 4, lax.rem(block, 4)
        cols = pl.ds(pl.multiple_of(block * 256, 256), 256)
        total = hmid[:, cols].astype(F32)
        for tt in range(2):
            w = buf[tt, zz, yy, :, :, pl.ds(DOWN, HALF_FF)].reshape(256, HALF_FF)
            total = total + dot_nt(hidden[:, tt * HALF_FF : tt * HALF_FF + HALF_FF], w)
        staged[block] = total.astype(BF16)
        out_copy(block, block).start()
        return carry

    over_rows(functools.partial(rms_rows, rows_in, norm_mix, normed))
    for number in range(1, 7):
        for flow in flows:
            flow.stage(number)
    for g in range(4):
        spatial_group(g)
    lax.fori_loop(0, 8, mix_out, 0)
    over_rows(functools.partial(rms_rows, hmid, norm_ffn, normed))
    for tt in range(2):
        lax.fori_loop(0, 11, gate_up(tt), 0)
    lax.fori_loop(0, 8, project_down, 0)
    for block in range(8):
        out_copy(block, block).wait()
    for flow in flows:
        for copy in flow.sent:
            copy.wait_send()


def on_device(
    tokens,
    norm_mix,
    w_unit,
    w_value,
    spatial,
    spatial_bias,
    group_gain,
    group_shift,
    w_mix_out,
    norm_ffn,
    w_gate,
    w_up,
    w_down,
):
    count, width = tokens.shape
    half = count // 2
    pairs = jnp.stack([w_gate.reshape(64, 11, 128), w_up.reshape(64, 11, 128)], axis=2)
    shard = jnp.concatenate(
        [w_unit, w_value, w_mix_out.T, pairs.reshape(64, 2816), w_down.T], axis=1
    )
    any_space = pl.BlockSpec(memory_space=pl.ANY)
    vmem = pl.BlockSpec(memory_space=pltpu.VMEM)
    return pl.pallas_call(
        kernel,
        out_shape=jax.ShapeDtypeStruct((half, width), BF16),
        in_specs=[any_space, any_space] + [vmem] * 6,
        out_specs=any_space,
        scratch_shapes=[
            pltpu.VMEM((2, 2, 4, 4, 64, WIDTH), BF16),
            pltpu.VMEM((half, width), BF16),
            pltpu.VMEM((half, width), BF16),
            pltpu.VMEM((half, 512), F32),
            pltpu.VMEM((half, 1024), BF16),
            pltpu.VMEM((half, width), BF16),
            pltpu.VMEM((half, 2 * HALF_FF), BF16),
            pltpu.VMEM((8, half, 256), BF16),
            pltpu.SemaphoreType.DMA((len(FLOWS), SENDS)),
            pltpu.SemaphoreType.DMA((len(FLOWS), SENDS)),
            pltpu.SemaphoreType.DMA((2,)),
            pltpu.SemaphoreType.DMA((8,)),
        ],
        compiler_params=pltpu.CompilerParams(
            collective_id=0, has_side_effects=True, vmem_limit_bytes=67043328
        ),
    )(
        tokens,
        shard,
        norm_mix.reshape(1, -1),
        spatial,
        spatial_bias.astype(F32)[:, :, None],
        group_gain.reshape(1, -1),
        group_shift.reshape(1, -1),
        norm_ffn.reshape(1, -1),
    )


def solution(mesh):
    placed = (
        P(("rep", "fs"), None),
        P(),
        P("fs", "tp"),
        P("fs", "tp"),
        P(),
        P(),
        P(),
        P(),
        P("tp", "fs"),
        P(),
        P("fs", "tp"),
        P("fs", "tp"),
        P("tp", "fs"),
    )
    return jax.shard_map(
        on_device,
        mesh=mesh,
        in_specs=placed,
        out_specs=P(("rep", "fs", "tp"), None),
        check_vma=False,
    )
```

time: 630 us -> 222 us (0.35)
  waiting for transfers between devices: 467 us -> 0 us
  Pallas kernels: 0 us -> 206 us
  matrix products: 51.8 us -> 0 us
  other arithmetic: 44.6 us -> 0.84 us
  blocking collectives: 28.2 us -> 0 us
  between operations: 13.3 us -> 0.07 us
  starting transfers between devices: 9.5 us -> 0 us
    all_gather x4 -> x0, waiting for transfers between devices: 467 us -> none  [the longest x2 270 us: sent_together(): lax.all_gather(both, axis, axis=dim, tiled=True)]
    pallas_call x0 -> x1, Pallas kernels: none -> 206 us  [on_device(): pl.pallas_call(kernel, out_shape=jax.ShapeDtypeStruct((half, width), BF16...]
    dot_general x5 -> x0, matrix products: 51.8 us -> none  [the longest x1 20.9 us: on_device(): jnp.dot(hidden, down_cols, preferred_element_type=jnp.float32)]
    reduce_sum x6 -> x0, other arithmetic: 39.2 us -> none  [the longest x1 14.4 us: spatial_unit(): spread = jnp.mean(jnp.square(active - center), axis=-1, keepdims=True)]
    all_to_all x1 -> x0, blocking collectives: 28.2 us -> none  [summed_on_arrival(): lax.all_to_all(pieces, axis, split_axis=0, concat_axis=0, tiled=True)]
    all_to_all x1 -> x0, starting transfers between devices: 9.34 us -> none  [sent_to_all(): return lax.all_to_all(copies, axis, split_axis=0, concat_axis=0, tiled=True)]
  transfers between devices with their start and end apart: 5 -> 0, of which waited for: 4 -> 0; matrix products, arithmetic and copies ran while one was open for 11% -> 0% of each run, Pallas kernels for 0% -> 0%
where the time goes in v1:
time: 222 us
  Pallas kernels  206 us (93%)
  local copies, waits for them, and re-layouts  15.2 us (7%)
    pallas_call x1, Pallas kernels, on_device(): pl.pallas_call(kernel, out_shape=jax.ShapeDtypeStruct((half, width), BF16...  206 us
    unnamed x13, local copies, waits for them, and re-layouts  5.84 us

profile of v1, /device:TPU:1, one launch (start us, length us, event | category | flops | bytes accessed | tf_op | source)
XLA Modules:
  0.0 221.9 jit_solution(6311144221728806709)
XLA Ops:
  0.0 0.0 copy-start.3
  0.0 0.7 bitcast_convert_fusion
  0.7 1.3 reshape.17.gain
  2.0 1.3 reshape.18.shift
  3.3 1.3 reshape.16.norm_mix
  4.6 1.3 reshape.19.norm_ffn
  5.9 0.9 copy.17.bias
  6.7 1.0 stack_reshape.6
  7.8 0.0 copy-start
  7.8 1.1 stack_reshape.7
  8.9 0.1 pad_maximum_fusion
  9.0 0.4 copy.16
  9.4 0.1 reshape.15
  9.5 0.0 copy-done.1
  9.6 0.6 constant_dynamic-update-slice_fusion.2
  10.2 0.0 copy-done.2
  10.2 0.6 constant_dynamic-update-slice_fusion.1
  10.8 0.0 copy-done.3
  10.8 0.6 bitcast_dynamic-update-slice_fusion.1
  11.5 0.8 constant_dynamic-update-slice_fusion
  12.2 0.0 copy-done
  12.2 0.7 bitcast_dynamic-update-slice_fusion.shard
  12.9 205.8 %shard_map.127 = bf16[512,2048]{1,0:T(8,128)(2,1)} custom-call(bf16[1024,2048]{1,0:T(8,128)(2,1)} %tokens.1, bf16[64,5760]{1,0:T(8,128)(2,1)} %bitcast_dynamic-update-slice_fusion.shard, bf16[1,2048]{1,0:T(2,128)(2,1)} %reshape.16.norm_mix, bf16[4,128,128]{2,1,0:T(8,128)(2,1)} %spatial.1, f32[4,128,1]{2,1,0:T(8,128)} %copy.17.bias, ...), custom_call_target="tpu_custom_call" | custom-call | tf_op jit(solution)/shard_map/pallas_call | solution.py:351
  218.8 3.2 %copy.23 = bf16[512,2048]{1,0:T(8,128)(2,1)} copy(bf16[512,2048]{1,0:T(8,128)(2,1)} %shard_map.127) | data formatting | bytes 4194304
  (2 shorter events, 0.0 us)
Async XLA Ops:
  0.0 10.8 %copy-start.3 = (bf16[512,64]{0,1:T(8,128)(2,1)S(1)}, bf16[512,64]{0,1:T(8,128)(2,1)}, u32[]{:S(2)}) copy-start(bf16[512,64]{0,1:T(8,128)(2,1)} %param.21) | copy-start | bytes 196612
  0.0 10.2 %copy-start.2 = (bf16[64,512]{1,0:T(8,128)(2,1)S(1)}, bf16[64,512]{1,0:T(8,128)(2,1)}, u32[]{:S(2)}) copy-start(bf16[64,512]{1,0:T(8,128)(2,1)} %param.16) | copy-start | bytes 196612
  0.0 9.5 %copy-start.1 = (bf16[64,512]{1,0:T(8,128)(2,1)S(1)}, bf16[64,512]{1,0:T(8,128)(2,1)}, u32[]{:S(2)}) copy-start(bf16[64,512]{1,0:T(8,128)(2,1)} %param.15) | copy-start | bytes 196612
  7.8 4.4 %copy-start = (bf16[1408,64]{0,1:T(8,128)(2,1)S(1)}, bf16[1408,64]{0,1:T(8,128)(2,1)}, u32[]{:S(2)}) copy-start(bf16[1408,64]{0,1:T(8,128)(2,1)} %param.25) | copy-start | bytes 540676

commit v2 on v1

v2 whole, which is shorter than its diff:
```python
import functools

import jax
import jax.numpy as jnp
from jax import lax
from jax.experimental import pallas as pl
from jax.experimental.pallas import tpu as pltpu
from jax.sharding import PartitionSpec as P

MESH = pl.DeviceIdType.MESH
F32 = jnp.float32
BF16 = jnp.bfloat16
LANES = 128

UNIT, VALUE, MIX, PAIRS, DOWN = 0, 512, 1024, 1536, 4352
WIDTH = 5760
HALF_FF = 1408

FLOWS = (
    (0, 3, "xyz"),
    (3, 3, "xzy"),
    (6, 2, "xyz"),
    (8, 2, "yxz"),
    (10, 2, "yzx"),
    (12, 4, "zyx"),
    (16, 4, "yxz"),
    (20, 4, "xyz"),
    (24, 4, "yzx"),
    (28, 3, "yxz"),
    (31, 3, "yxz"),
    (34, 3, "xzy"),
    (37, 2, "xzy"),
    (39, 2, "xzy"),
    (41, 2, "zyx"),
    (43, 2, "xyz"),
)
DOWN_PARTS = (
    (0, 896),
    (896, 512),
)
SCHEDULE = (
    ("s", 0, 0),
    ("s", 3, 0),
    ("s", 10, 0),
    ("n1",),
    ("s", 2, 0),
    ("s", 1, 0),
    ("s", 8, 0),
    ("s", 3, 1),
    ("s", 0, 1),
    ("s", 7, 0),
    ("s", 10, 1),
    ("s", 2, 1),
    ("s", 4, 0),
    ("s", 1, 1),
    ("s", 8, 1),
    ("s", 3, 2),
    ("s", 0, 2),
    ("s", 11, 0),
    ("s", 10, 2),
    ("s", 7, 1),
    ("s", 4, 1),
    ("s", 2, 2),
    ("s", 1, 2),
    ("s", 8, 2),
    ("s", 3, 3),
    ("s", 12, 0),
    ("s", 11, 1),
    ("s", 0, 3),
    ("s", 1, 3),
    ("s", 4, 2),
    ("s", 6, 0),
    ("s", 8, 3),
    ("s", 2, 3),
    ("s", 10, 3),
    ("s", 7, 2),
    ("s", 13, 0),
    ("s", 4, 3),
    ("s", 0, 4),
    ("s", 3, 4),
    ("s", 9, 0),
    ("s", 5, 0),
    ("s", 12, 1),
    ("s", 11, 2),
    ("s", 1, 4),
    ("s", 6, 1),
    ("s", 0, 5),
    ("s", 2, 4),
    ("s", 8, 4),
    ("s", 10, 4),
    ("s", 0, 6),
    ("s", 13, 1),
    ("s", 3, 5),
    ("s", 7, 3),
    ("s", 5, 1),
    ("s", 9, 1),
    ("s", 11, 3),
    ("s", 4, 4),
    ("s", 12, 2),
    ("s", 1, 5),
    ("s", 6, 2),
    ("s", 3, 6),
    ("s", 2, 5),
    ("s", 7, 4),
    ("s", 14, 0),
    ("s", 8, 5),
    ("s", 13, 2),
    ("s", 5, 2),
    ("s", 9, 2),
    ("s", 1, 6),
    ("g", 0),
    ("s", 2, 6),
    ("s", 4, 5),
    ("g", 1),
    ("s", 10, 5),
    ("s", 12, 3),
    ("g", 2),
    ("s", 6, 3),
    ("s", 8, 6),
    ("s", 11, 4),
    ("s", 4, 6),
    ("s", 15, 0),
    ("g", 3),
    ("s", 5, 3),
    ("s", 10, 6),
    ("s", 9, 3),
    ("m", 0, 4),
    ("s", 6, 4),
    ("m", 4, 6),
    ("s", 12, 4),
    ("s", 15, 1),
    ("m", 6, 8),
    ("n2",),
    ("s", 14, 1),
    ("s", 7, 5),
    ("u", 0, 4, 2),
    ("s", 13, 3),
    ("s", 11, 5),
    ("u", 0, 6, 2),
    ("u", 1, 6, 2),
    ("s", 12, 5),
    ("s", 14, 2),
    ("s", 7, 6),
    ("u", 1, 4, 2),
    ("s", 5, 4),
    ("s", 11, 6),
    ("s", 12, 6),
    ("s", 9, 4),
    ("s", 15, 2),
    ("s", 13, 4),
    ("s", 6, 5),
    ("s", 14, 3),
    ("u", 0, 2, 2),
    ("s", 15, 3),
    ("s", 5, 5),
    ("u", 0, 0, 2),
    ("s", 13, 5),
    ("s", 15, 4),
    ("s", 6, 6),
    ("u", 1, 2, 2),
    ("s", 14, 4),
    ("s", 9, 5),
    ("u", 0, 8, 3),
    ("s", 5, 6),
    ("s", 13, 6),
    ("u", 1, 0, 2),
    ("d", 0, 0, 4),
    ("s", 14, 5),
    ("s", 15, 5),
    ("d", 0, 4, 6),
    ("s", 9, 6),
    ("u", 1, 8, 3),
    ("s", 14, 6),
    ("d", 0, 6, 8),
    ("s", 15, 6),
    ("d", 1, 0, 8),
)
SENDS = 14


class Flow:
    def __init__(self, index, buf, send_sems, recv_sems, where):
        first, tiles, order = FLOWS[index]
        self.index = index
        self.cols = pl.ds(first * LANES, tiles * LANES)
        self.buf, self.send_sems, self.recv_sems = buf, send_sems, recv_sems
        self.core, self.home, self.to = where
        self.sent = []
        self.stages = self.plan(order)

    def part(self, place, rows, core):
        row = (pl.ds(0, 64), pl.ds(0, 32), pl.ds(32, 32))[rows]
        at = [slice(None) if place[a] is None else place[a] for a in "zyx"]
        return self.buf.at[core, at[0], at[1], at[2], row, self.cols]

    def copy(self, slot, ref, device):
        return pltpu.make_async_remote_copy(
            src_ref=ref,
            dst_ref=ref,
            send_sem=self.send_sems.at[self.index, slot],
            recv_sem=self.recv_sems.at[self.index, slot],
            device_id=self.to[device],
            device_id_type=MESH,
        )

    def send(self, slot, place, rows, device):
        copy = self.copy(slot, self.part(place, rows, self.core), device)
        copy.start()
        self.sent.append(copy)

    def arrived(self, slot, place, rows, device):
        core = 1 - self.core if device == "core" else self.core
        self.copy(slot, self.part(place, rows, core), device).wait_recv()

    def stage(self, number):
        for action, args in self.stages[number]:
            action(*args)

    def plan(self, order):
        stages, slot, arrivals = [], 0, []
        place = dict(self.home)
        relay = []
        for axis in order:
            last = axis == order[2]
            shift = lambda d, p=place, a=axis: {
                **p, a: lax.rem(p[a] + d, 2 if a == "z" else 4)
            }
            plus, minus = axis + "+", axis + "-"
            own = place
            if axis == "z":
                now = list(arrivals)
                now.append((self.send, (slot, own, 1, plus)))
                now.append((self.send, (slot + 1, own, 2, minus)))
                other = shift(1)
                arrivals = [
                    (self.arrived, (slot, other, 1, minus)),
                    (self.arrived, (slot + 1, other, 2, plus)),
                ]
                slot += 2
                if last:
                    now.append((self.send, (10, own, 0, "core")))
                stages.append(now)
                if last:
                    stages.append(arrivals + [(self.send, (11, other, 0, "core"))])
                    relay = [(10, own), (11, other)]
            else:
                now = list(arrivals)
                now.append((self.send, (slot, own, 0, plus)))
                now.append((self.send, (slot + 1, own, 0, minus)))
                if last:
                    now.append((self.send, (10, own, 0, "core")))
                stages.append(now)
                before, after, far = shift(3), shift(1), shift(2)
                now = [
                    (self.arrived, (slot, before, 0, minus)),
                    (self.send, (slot + 2, before, 1, plus)),
                    (self.arrived, (slot + 1, after, 0, plus)),
                    (self.send, (slot + 3, after, 2, minus)),
                ]
                if last:
                    now.append((self.send, (11, before, 0, "core")))
                    now.append((self.send, (12, after, 0, "core")))
                stages.append(now)
                arrivals = [
                    (self.arrived, (slot + 2, far, 1, minus)),
                    (self.arrived, (slot + 3, far, 2, plus)),
                ]
                if last:
                    stages.append(arrivals + [(self.send, (13, far, 0, "core"))])
                    relay = [(10, own), (11, before), (12, after), (13, far)]
                slot += 4
            place = {**place, axis: None}
        stages.append([(self.arrived, (n, p, 0, "core")) for n, p in relay])
        return stages


def rms_rows(source, gain, target, rows):
    values = source[rows, :].astype(F32)
    scale = lax.rsqrt(jnp.mean(values * values, axis=-1, keepdims=True) + 1e-06)
    target[rows, :] = (values * scale * gain[...].astype(F32)).astype(BF16)


def dot(a, b):
    return jnp.dot(a, b, preferred_element_type=F32)


def dot_nt(a, b):
    return lax.dot_general(a, b, (((1,), (1,)), ((), ())), preferred_element_type=F32)


def kernel(
    tokens,
    shard,
    norm_mix,
    spatial,
    bias,
    gain,
    shift,
    norm_ffn,
    out,
    buf,
    rows_in,
    normed,
    pre,
    gated,
    hmid,
    hidden,
    acc,
    staged,
    send_sems,
    recv_sems,
    local_sems,
    out_sems,
):
    r, f, t = lax.axis_index("rep"), lax.axis_index("fs"), lax.axis_index("tp")
    z, y, x = f // 16, lax.rem(f // 4, 4), lax.rem(f, 4)
    up, down = lax.rem(2 * r + z + 1, 4), lax.rem(2 * r + z + 3, 4)
    at = lambda zz, yy, xx, tt: (zz // 2, lax.rem(zz, 2) * 16 + yy * 4 + xx, tt)
    here = 2 * r + z
    to = {
        "x+": at(here, y, lax.rem(x + 1, 4), t),
        "x-": at(here, y, lax.rem(x + 3, 4), t),
        "y+": at(here, lax.rem(y + 1, 4), x, t),
        "y-": at(here, lax.rem(y + 3, 4), x, t),
        "z+": at(up, y, x, t),
        "z-": at(down, y, x, t),
        "core": at(here, y, x, 1 - t),
    }

    own = pltpu.make_async_copy(shard, buf.at[t, z, y, x], local_sems.at[0])
    own.start()
    count = rows_in.shape[0]
    load = pltpu.make_async_copy(
        tokens.at[pl.ds(t * count, count)], rows_in, local_sems.at[1]
    )
    load.start()

    barrier = pltpu.get_barrier_semaphore()
    for device in to.values():
        pl.semaphore_signal(barrier, inc=1, device_id=device, device_id_type=MESH)
    pl.semaphore_wait(barrier, len(to))
    own.wait()

    where = (t, {"z": z, "y": y, "x": x}, to)
    flows = [Flow(i, buf, send_sems, recv_sems, where) for i in range(len(FLOWS))]

    blocks = count // LANES

    def over_rows(body):
        def step(i, carry):
            body(pl.ds(pl.multiple_of(i * LANES, LANES), LANES))
            return carry

        lax.fori_loop(0, blocks, step, 0)

    def columns(tt, first, size):
        return buf[tt, :, :, :, :, pl.ds(first, size)].reshape(2048, size)

    def spatial_group(g):
        tt, low = g // 2, (g % 2) * 256
        pre[:, 0:256] = dot(normed[...], columns(tt, UNIT + low, 256))
        pre[:, 256:512] = dot(normed[...], columns(tt, VALUE + low, 256))
        at_row = lax.broadcasted_iota(jnp.int32, (128, 128), 0)
        at_col = lax.broadcasted_iota(jnp.int32, (128, 128), 1)
        weights = jnp.where(at_row >= at_col, spatial[g], jnp.zeros((128, 128), BF16))
        g_gain = gain[:, g * 256 : g * 256 + 256].astype(F32)
        g_shift = shift[:, g * 256 : g * 256 + 256].astype(F32)

        def body(rows):
            active = jax.nn.gelu(pre[rows, 256:512], approximate=True)
            center = jnp.mean(active, axis=-1, keepdims=True)
            off = active - center
            spread = jnp.mean(off * off, axis=-1, keepdims=True)
            grouped = off * lax.rsqrt(spread + 1e-06) * g_gain + g_shift
            mixed = dot(weights, grouped.astype(BF16)) + bias[g]
            value = jax.nn.gelu(pre[rows, 0:256], approximate=True) * mixed
            gated[rows, g * 256 : g * 256 + 256] = value.astype(BF16)

        over_rows(body)

    def mix_out(block, carry):
        zz, yy = block // 4, lax.rem(block, 4)
        cols = pl.ds(pl.multiple_of(block * 256, 256), 256)
        total = rows_in[:, cols].astype(F32)
        for tt in range(2):
            w = buf[tt, zz, yy, :, :, pl.ds(MIX, 512)].reshape(256, 512)
            total = total + dot_nt(gated[:, tt * 512 : tt * 512 + 512], w)
        hmid[:, cols] = total.astype(BF16)
        return carry

    def gate_up(tt, pair, pairs):
        def step(i, carry):
            first = pl.multiple_of(PAIRS + i * 256, 256)
            both = dot(normed[...], columns(tt, first, 256))
            value = jax.nn.silu(both[:, 0:128]) * both[:, 128:256]
            into = pl.ds(pl.multiple_of(tt * HALF_FF + i * 128, 128), 128)
            hidden[:, into] = value.astype(BF16)
            return carry

        lax.fori_loop(pair, pair + pairs, step, 0)

    def out_copy(block):
        cols = pl.ds(pl.multiple_of(block * 256, 256), 256)
        return pltpu.make_async_copy(staged.at[block], out.at[:, cols], out_sems.at[block])

    def project_down(part):
        first, size = DOWN_PARTS[part]

        def step(block, carry):
            zz, yy = block // 4, lax.rem(block, 4)
            cols = pl.ds(pl.multiple_of(block * 256, 256), 256)
            total = acc[block] if part else hmid[:, cols].astype(F32)
            for tt in range(2):
                w = buf[tt, zz, yy, :, :, pl.ds(DOWN + first, size)].reshape(256, size)
                a = hidden[:, tt * HALF_FF + first : tt * HALF_FF + first + size]
                total = total + dot_nt(a, w)
            if part == len(DOWN_PARTS) - 1:
                staged[block] = total.astype(BF16)
                out_copy(block).start()
            else:
                acc[block] = total
            return carry

        return step

    def run(op, *args):
        if op == "s":
            flows[args[0]].stage(args[1])
        elif op == "n1":
            load.wait()
            over_rows(functools.partial(rms_rows, rows_in, norm_mix, normed))
        elif op == "n2":
            over_rows(functools.partial(rms_rows, hmid, norm_ffn, normed))
        elif op == "g":
            spatial_group(args[0])
        elif op == "m":
            lax.fori_loop(args[0], args[1], mix_out, 0)
        elif op == "u":
            gate_up(lax.rem(t + args[0], 2), args[1], args[2])
        else:
            lax.fori_loop(args[1], args[2], project_down(args[0]), 0)

    for item in SCHEDULE:
        run(*item)
    for block in range(8):
        out_copy(block).wait()
    for flow in flows:
        for copy in flow.sent:
            copy.wait_send()


def on_device(
    tokens,
    norm_mix,
    w_unit,
    w_value,
    spatial,
    spatial_bias,
    group_gain,
    group_shift,
    w_mix_out,
    norm_ffn,
    w_gate,
    w_up,
    w_down,
):
    count, width = tokens.shape
    half = count // 2
    pairs = jnp.stack([w_gate.reshape(64, 11, 128), w_up.reshape(64, 11, 128)], axis=2)
    shard = jnp.concatenate(
        [w_unit, w_value, w_mix_out.T, pairs.reshape(64, 2816), w_down.T], axis=1
    )
    any_space = pl.BlockSpec(memory_space=pl.ANY)
    vmem = pl.BlockSpec(memory_space=pltpu.VMEM)
    return pl.pallas_call(
        kernel,
        out_shape=jax.ShapeDtypeStruct((half, width), BF16),
        in_specs=[any_space, any_space] + [vmem] * 6,
        out_specs=any_space,
        scratch_shapes=[
            pltpu.VMEM((2, 2, 4, 4, 64, WIDTH), BF16),
            pltpu.VMEM((half, width), BF16),
            pltpu.VMEM((half, width), BF16),
            pltpu.VMEM((half, 512), F32),
            pltpu.VMEM((half, 1024), BF16),
            pltpu.VMEM((half, width), BF16),
            pltpu.VMEM((half, 2 * HALF_FF), BF16),
            pltpu.VMEM((8, half, 256), F32),
            pltpu.VMEM((8, half, 256), BF16),
            pltpu.SemaphoreType.DMA((len(FLOWS), SENDS)),
            pltpu.SemaphoreType.DMA((len(FLOWS), SENDS)),
            pltpu.SemaphoreType.DMA((2,)),
            pltpu.SemaphoreType.DMA((8,)),
        ],
        compiler_params=pltpu.CompilerParams(
            collective_id=0, has_side_effects=True, vmem_limit_bytes=67043328
        ),
    )(
        tokens,
        shard,
        norm_mix.reshape(1, -1),
        spatial,
        spatial_bias.astype(F32)[:, :, None],
        group_gain.reshape(1, -1),
        group_shift.reshape(1, -1),
        norm_ffn.reshape(1, -1),
    )


def solution(mesh):
    placed = (
        P(("rep", "fs"), None),
        P(),
        P("fs", "tp"),
        P("fs", "tp"),
        P(),
        P(),
        P(),
        P(),
        P("tp", "fs"),
        P(),
        P("fs", "tp"),
        P("fs", "tp"),
        P("tp", "fs"),
    )
    return jax.shard_map(
        on_device,
        mesh=mesh,
        in_specs=placed,
        out_specs=P(("rep", "fs", "tp"), None),
        check_vma=False,
    )
```

time: 222 us -> 133 us (0.60)
  Pallas kernels: 206 us -> 115 us
    pallas_call x1, Pallas kernels: 206 us -> 115 us  [on_device(): pl.pallas_call(kernel, out_shape=jax.ShapeDtypeStruct((half, width), BF16...]
where the time goes in v2:
time: 133 us; the launch traced here: 131 us
  Pallas kernels  115 us (86%)
  local copies, waits for them, and re-layouts  15.2 us (11%)
    pallas_call x1, Pallas kernels, on_device(): pl.pallas_call(kernel, out_shape=jax.ShapeDtypeStruct((half, width), BF16...  115 us
    unnamed x13, local copies, waits for them, and re-layouts  5.84 us

profile of v2, /device:TPU:1, one launch (start us, length us, event | category | flops | bytes accessed | tf_op | source)
XLA Modules:
  0.0 130.9 jit_solution(14660458095812105111)
XLA Ops:
  0.0 0.0 copy-start.3
  0.0 0.7 bitcast_convert_fusion
  0.7 1.3 reshape.17.gain
  2.0 1.3 reshape.18.shift
  3.3 1.3 reshape.16.norm_mix
  4.6 1.3 reshape.19.norm_ffn
  5.9 0.9 copy.17.bias
  6.7 1.0 stack_reshape.6
  7.8 0.0 copy-start
  7.8 1.1 stack_reshape.7
  8.9 0.1 pad_maximum_fusion
  9.0 0.4 copy.16
  9.4 0.1 reshape.15
  9.5 0.0 copy-done.1
  9.6 0.6 constant_dynamic-update-slice_fusion.2
  10.2 0.0 copy-done.2
  10.2 0.6 constant_dynamic-update-slice_fusion.1
  10.8 0.0 copy-done.3
  10.8 0.6 bitcast_dynamic-update-slice_fusion.1
  11.5 0.8 constant_dynamic-update-slice_fusion
  12.2 0.0 copy-done
  12.2 0.7 bitcast_dynamic-update-slice_fusion.shard
  12.9 114.8 %shard_map.127 = bf16[512,2048]{1,0:T(8,128)(2,1)} custom-call(bf16[1024,2048]{1,0:T(8,128)(2,1)} %tokens.1, bf16[64,5760]{1,0:T(8,128)(2,1)} %bitcast_dynamic-update-slice_fusion.shard, bf16[1,2048]{1,0:T(2,128)(2,1)} %reshape.16.norm_mix, bf16[4,128,128]{2,1,0:T(8,128)(2,1)} %spatial.1, f32[4,128,1]{2,1,0:T(8,128)} %copy.17.bias, ...), custom_call_target="tpu_custom_call" | custom-call | tf_op jit(solution)/shard_map/pallas_call | solution.py:475
  127.7 3.2 %copy.23 = bf16[512,2048]{1,0:T(8,128)(2,1)} copy(bf16[512,2048]{1,0:T(8,128)(2,1)} %shard_map.127) | data formatting | bytes 4194304
  (2 shorter events, 0.0 us)
Async XLA Ops:
  0.0 10.8 %copy-start.3 = (bf16[512,64]{0,1:T(8,128)(2,1)S(1)}, bf16[512,64]{0,1:T(8,128)(2,1)}, u32[]{:S(2)}) copy-start(bf16[512,64]{0,1:T(8,128)(2,1)} %param.21) | copy-start | bytes 196612
  0.0 10.2 %copy-start.2 = (bf16[64,512]{1,0:T(8,128)(2,1)S(1)}, bf16[64,512]{1,0:T(8,128)(2,1)}, u32[]{:S(2)}) copy-start(bf16[64,512]{1,0:T(8,128)(2,1)} %param.16) | copy-start | bytes 196612
  0.0 9.5 %copy-start.1 = (bf16[64,512]{1,0:T(8,128)(2,1)S(1)}, bf16[64,512]{1,0:T(8,128)(2,1)}, u32[]{:S(2)}) copy-start(bf16[64,512]{1,0:T(8,128)(2,1)} %param.15) | copy-start | bytes 196612
  7.8 4.4 %copy-start = (bf16[1408,64]{0,1:T(8,128)(2,1)S(1)}, bf16[1408,64]{0,1:T(8,128)(2,1)}, u32[]{:S(2)}) copy-start(bf16[1408,64]{0,1:T(8,128)(2,1)} %param.25) | copy-start | bytes 540676

commit v3 on v0

v3 whole, which is shorter than its diff:
```python
import functools

import jax
import jax.numpy as jnp
from jax import lax
from jax.experimental import pallas as pl
from jax.experimental.pallas import tpu as pltpu
from jax.sharding import PartitionSpec as P

MESH = pl.DeviceIdType.MESH
F32 = jnp.float32
BF16 = jnp.bfloat16
LANES = 128

MIX, PAIRS, DOWN = 1024, 1536, 4352
WIDTH = 5760
HALF_FF = 1408

FLOWS = (
    (0, 2, "yzx"),
    (2, 2, "yxz"),
    (4, 1, "yzx"),
    (5, 3, "xyz"),
    (8, 1, "yxz"),
    (9, 3, "yxz"),
    (12, 4, "xzy"),
    (16, 6, "xzy"),
    (22, 6, "yxz"),
    (28, 4, "xzy"),
    (32, 2, "xyz"),
    (34, 4, "yzx"),
    (38, 4, "yxz"),
    (42, 3, "yzx"),
)
DOWN_PARTS = (
    (0, 512),
    (512, 512),
    (1024, 384),
)
SCHEDULE = (
    ("s", 3, 0),
    ("s", 5, 0),
    ("s", 7, 0),
    ("s", 1, 0),
    ("s", 2, 0),
    ("s", 0, 0),
    ("n1",),
    ("s", 6, 0),
    ("s", 3, 1),
    ("s", 5, 1),
    ("s", 4, 0),
    ("s", 1, 1),
    ("s", 2, 1),
    ("s", 0, 1),
    ("s", 8, 0),
    ("s", 7, 1),
    ("s", 5, 2),
    ("s", 4, 1),
    ("s", 1, 2),
    ("s", 2, 2),
    ("s", 6, 1),
    ("s", 10, 0),
    ("s", 3, 2),
    ("s", 0, 2),
    ("s", 7, 2),
    ("s", 2, 3),
    ("s", 8, 1),
    ("s", 4, 2),
    ("s", 0, 3),
    ("s", 5, 3),
    ("s", 9, 0),
    ("s", 11, 0),
    ("s", 12, 0),
    ("s", 3, 3),
    ("s", 8, 2),
    ("s", 7, 3),
    ("s", 1, 3),
    ("s", 6, 2),
    ("s", 11, 1),
    ("s", 10, 1),
    ("s", 13, 0),
    ("s", 12, 1),
    ("s", 2, 4),
    ("s", 3, 4),
    ("s", 6, 3),
    ("s", 4, 3),
    ("s", 0, 4),
    ("s", 5, 4),
    ("s", 3, 5),
    ("s", 3, 6),
    ("s", 9, 1),
    ("s", 3, 7),
    ("s", 7, 4),
    ("s", 11, 2),
    ("s", 13, 1),
    ("s", 8, 3),
    ("s", 5, 5),
    ("s", 5, 6),
    ("s", 12, 2),
    ("s", 1, 4),
    ("s", 10, 2),
    ("s", 2, 5),
    ("s", 11, 3),
    ("s", 4, 4),
    ("s", 5, 7),
    ("s", 2, 7),
    ("g", 1),
    ("s", 9, 2),
    ("s", 1, 5),
    ("s", 1, 6),
    ("s", 0, 5),
    ("g", 3),
    ("s", 6, 4),
    ("s", 1, 7),
    ("s", 4, 5),
    ("s", 8, 4),
    ("s", 4, 6),
    ("s", 0, 7),
    ("g", 0),
    ("s", 9, 3),
    ("g", 2),
    ("s", 12, 3),
    ("s", 4, 7),
    ("m", 0, 0, 4),
    ("s", 7, 5),
    ("m", 1, 0, 2),
    ("s", 13, 2),
    ("m", 1, 2, 4),
    ("n2",),
    ("s", 10, 3),
    ("s", 7, 7),
    ("u", 0, 2, 2),
    ("u", 1, 2, 2),
    ("s", 11, 4),
    ("s", 6, 5),
    ("u", 0, 0, 2),
    ("s", 12, 4),
    ("s", 8, 5),
    ("s", 8, 6),
    ("u", 0, 4, 2),
    ("u", 0, 6, 2),
    ("s", 6, 7),
    ("s", 13, 3),
    ("u", 1, 0, 2),
    ("s", 11, 5),
    ("s", 8, 7),
    ("u", 1, 4, 2),
    ("s", 9, 4),
    ("u", 1, 6, 2),
    ("s", 10, 4),
    ("s", 11, 7),
    ("d", 0, 0, 0, 4),
    ("d", 0, 1, 0, 2),
    ("s", 12, 5),
    ("s", 12, 6),
    ("s", 13, 4),
    ("d", 0, 1, 2, 4),
    ("d", 1, 0, 0, 4),
    ("s", 9, 5),
    ("s", 12, 7),
    ("d", 1, 1, 0, 4),
    ("s", 10, 5),
    ("s", 10, 6),
    ("u", 0, 8, 3),
    ("s", 9, 7),
    ("s", 13, 5),
    ("s", 10, 7),
    ("u", 1, 8, 3),
    ("s", 13, 7),
    ("d", 2, 0, 0, 4),
    ("d", 2, 1, 0, 4),
)
class Flow:
    def __init__(self, index, buf, send_sems, recv_sems, where):
        first, tiles, order = FLOWS[index]
        self.index = index
        self.cols = pl.ds(first * LANES, tiles * LANES)
        self.buf, self.send_sems, self.recv_sems = buf, send_sems, recv_sems
        self.core, self.home, self.to = where
        self.sent = []
        self.stages = self.plan(order)

    def part(self, place, rows, core):
        row = (pl.ds(0, 64), pl.ds(0, 32), pl.ds(32, 32))[rows]
        at = [slice(None) if place[a] is None else place[a] for a in "zyx"]
        return self.buf.at[core, at[0], at[1], at[2], row, self.cols]

    def copy(self, sems, ref, device):
        return pltpu.make_async_remote_copy(
            src_ref=ref,
            dst_ref=ref,
            send_sem=self.send_sems.at[self.index, sems[0]],
            recv_sem=self.recv_sems.at[self.index, sems[1]],
            device_id=self.to[device],
            device_id_type=MESH,
        )

    def send(self, sems, place, rows, device):
        self.copy(sems, self.part(place, rows, self.core), device).start()

    def arrived(self, sems, place, core=0):
        core = 1 - self.core if core else self.core
        self.copy(sems, self.part(place, 0, core), "core").wait_recv()

    def finish(self):
        for sem, place in self.sent:
            self.copy((sem, 0), self.part(place, 0, self.core), "core").wait_send()

    def stage(self, number):
        for action, *args in self.stages[number]:
            action(*args)

    def plan(self, order):
        send, arrived = self.send, self.arrived
        stages, recv, arrivals = [], 0, []
        place = dict(self.home)
        every = dict.fromkeys("zyx")
        for phase, axis in enumerate(order):
            last = phase == 2
            put = lambda v, p=place, a=axis: {**p, a: v}
            shift = lambda d, p=place, a=axis: put(lax.rem(p[a] + d, 2 if a == "z" else 4))
            plus, minus = axis + "+", axis + "-"
            one, two, relay = (phase, recv), (phase, recv + 1), (3, 5)
            if axis == "z":
                recv += 1
                other = shift(1)
                now = arrivals + [(send, one, place, 1, plus), (send, one, place, 2, minus)]
                arrivals = [(arrived, one, other)]
                self.sent.append((phase, place))
                if last:
                    now.append((send, relay, place, 0, "core"))
                    after = arrivals + [(send, (3, 6), other, 0, "core")]
                    stages += [now, after]
                    stages.append([(arrived, relay, place, 1)])
                    stages.append([(arrived, (3, 6), other, 1)])
                else:
                    stages.append(now)
            else:
                recv += 2
                now = arrivals + [(send, one, place, 0, plus), (send, one, place, 0, minus)]
                before, after, far = shift(3), shift(1), shift(2)
                then = [
                    (arrived, one, put(pl.ds(0, 2))),
                    (send, two, before, 1, plus),
                    (send, two, after, 2, minus),
                ]
                arrivals = [(arrived, two, far)]
                self.sent.append((phase, put(pl.ds(0, 3))))
                stages += [now, then]
                if last:
                    now.append((send, relay, place, 0, "core"))
                    then.append((send, relay, before, 0, "core"))
                    then.append((send, relay, after, 0, "core"))
                    stages.append(arrivals + [(send, relay, far, 0, "core")])
                    stages.append([])
                    stages.append([(arrived, relay, every, 1)])
            place = {**place, axis: None}
        self.sent.append((3, every))
        return stages


def rms_rows(source, gain, target, rows):
    values = source[rows, :].astype(F32)
    scale = lax.rsqrt(jnp.mean(values * values, axis=-1, keepdims=True) + 1e-06)
    target[rows, :] = (values * scale * gain[...].astype(F32)[None, :]).astype(BF16)


def dot(a, b):
    return jnp.dot(a, b, preferred_element_type=F32)


def dot_nt(a, b):
    return lax.dot_general(a, b, (((1,), (1,)), ((), ())), preferred_element_type=F32)


def kernel(
    tokens,
    w_unit,
    w_value,
    mix_rows,
    w_gate,
    w_up,
    down_rows,
    norm_mix_in,
    spatial_in,
    bias_in,
    gain_in,
    shift_in,
    norm_ffn_in,
    out,
    buf,
    rows_in,
    normed,
    pre,
    gated,
    hidden,
    acc,
    send_sems,
    recv_sems,
    norm_mix,
    spatial,
    bias,
    gain,
    shift,
    norm_ffn,
    local_sems,
):
    r, f, t = lax.axis_index("rep"), lax.axis_index("fs"), lax.axis_index("tp")
    z, y, x = f // 16, lax.rem(f // 4, 4), lax.rem(f, 4)
    up, down = lax.rem(2 * r + z + 1, 4), lax.rem(2 * r + z + 3, 4)
    at = lambda zz, yy, xx, tt: (zz // 2, lax.rem(zz, 2) * 16 + yy * 4 + xx, tt)
    here = 2 * r + z
    to = {
        "x+": at(here, y, lax.rem(x + 1, 4), t),
        "x-": at(here, y, lax.rem(x + 3, 4), t),
        "y+": at(here, lax.rem(y + 1, 4), x, t),
        "y-": at(here, lax.rem(y + 3, 4), x, t),
        "z+": at(up, y, x, t),
        "z-": at(down, y, x, t),
        "core": at(here, y, x, 1 - t),
    }

    barrier = pltpu.get_barrier_semaphore()
    for device in to.values():
        pl.semaphore_signal(barrier, inc=1, device_id=device, device_id_type=MESH)

    mine = buf.at[t, z, y, x]

    def load_own(source, first, size, slot):
        place = mine.at[:, pl.ds(first, size)]
        pltpu.make_async_copy(source, place, local_sems.at[slot]).start()

    for low in range(0, 512, 256):
        half = pl.ds(low, 256)
        load_own(w_unit.at[:, half], 2 * low, 256, 0)
        load_own(w_value.at[:, half], 2 * low + 256, 256, 0)
    load_own(mix_rows, MIX, 512, 0)
    for i in range(HALF_FF // LANES):
        for source, first in ((w_gate, PAIRS), (w_up, PAIRS + LANES)):
            load_own(source.at[:, pl.ds(i * LANES, LANES)], first + 2 * i * LANES, LANES, 2)
    load_own(down_rows, DOWN, HALF_FF, 2)

    def own_ready(first, size, slot):
        place = mine.at[:, pl.ds(first, size)]
        pltpu.make_async_copy(place, place, local_sems.at[slot]).wait()

    count = rows_in.shape[0]
    load = pltpu.make_async_copy(
        tokens.at[pl.ds(t * count, count)], rows_in, local_sems.at[1]
    )
    load.start()
    small = [
        pltpu.make_async_copy(source, target, local_sems.at[3 + i])
        for i, (source, target) in enumerate(
            (
                (norm_mix_in, norm_mix),
                (spatial_in, spatial),
                (bias_in, bias),
                (gain_in, gain),
                (shift_in, shift),
                (norm_ffn_in, norm_ffn),
            )
        )
    ]
    for copy in small:
        copy.start()

    pl.semaphore_wait(barrier, len(to))
    own_ready(0, PAIRS, 0)
    own_ready(PAIRS, WIDTH - PAIRS, 2)

    where = (t, {"z": z, "y": y, "x": x}, to)
    flows = [Flow(i, buf, send_sems, recv_sems, where) for i in range(len(FLOWS))]

    blocks = count // LANES

    def over_rows(body):
        def step(i, carry):
            body(pl.ds(pl.multiple_of(i * LANES, LANES), LANES))
            return carry

        lax.fori_loop(0, blocks, step, 0)

    def columns(tt, first, size):
        return buf[tt, :, :, :, :, pl.ds(first, size)].reshape(2048, size)

    def spatial_group(g):
        tt, low = g // 2, (g % 2) * 256
        pre[...] = dot(normed[...], columns(tt, 2 * low, 512))
        at_row = lax.broadcasted_iota(jnp.int32, (128, 128), 0)
        at_col = lax.broadcasted_iota(jnp.int32, (128, 128), 1)
        weights = jnp.where(at_row >= at_col, spatial[g], jnp.zeros((128, 128), BF16))
        lift = jnp.transpose(jnp.broadcast_to(bias[g : g + 1, :].astype(F32), (128, 128)))
        lift = jnp.concatenate([lift, lift], axis=1)
        g_gain = gain[pl.ds(g * 256, 256)].astype(F32)[None, :]
        g_shift = shift[pl.ds(g * 256, 256)].astype(F32)[None, :]

        def body(rows):
            active = jax.nn.gelu(pre[rows, 256:512], approximate=True)
            center = jnp.mean(active, axis=-1, keepdims=True)
            off = active - center
            spread = jnp.mean(off * off, axis=-1, keepdims=True)
            grouped = off * lax.rsqrt(spread + 1e-06) * g_gain + g_shift
            mixed = dot(weights, grouped.astype(BF16)) + lift
            value = jax.nn.gelu(pre[rows, 0:256], approximate=True) * mixed
            gated[rows, g * 256 : g * 256 + 256] = value.astype(BF16)

        over_rows(body)

    def mix_out(zz, yy):
        block = zz * 4 + yy
        cols = pl.ds(pl.multiple_of(block * 256, 256), 256)
        total = rows_in[:, cols].astype(F32)
        for tt in range(2):
            w = buf[tt, zz, yy, :, :, pl.ds(MIX, 512)].reshape(256, 512)
            total = total + dot_nt(gated[:, tt * 512 : tt * 512 + 512], w)
        rows_in[:, cols] = total.astype(BF16)

    def gate_up(tt, pair, pairs):
        def step(i, carry):
            first = pl.multiple_of(PAIRS + i * 256, 256)
            both = dot(normed[...], columns(tt, first, 256))
            value = jax.nn.silu(both[:, 0:128]) * both[:, 128:256]
            into = pl.ds(pl.multiple_of(tt * HALF_FF + i * 128, 128), 128)
            hidden[:, into] = value.astype(BF16)
            return carry

        lax.fori_loop(pair, pair + pairs, step, 0)

    def project_down(part, zz, yy):
        first, size = DOWN_PARTS[part]
        block = zz * 4 + yy
        cols = pl.ds(pl.multiple_of(block * 256, 256), 256)
        total = acc[block] if part else rows_in[:, cols].astype(F32)
        for tt in range(2):
            w = buf[tt, zz, yy, :, :, pl.ds(DOWN + first, size)].reshape(256, size)
            a = hidden[:, tt * HALF_FF + first : tt * HALF_FF + first + size]
            total = total + dot_nt(a, w)
        if part == len(DOWN_PARTS) - 1:
            out[:, cols] = total.astype(BF16)
        else:
            acc[block] = total

    def over_blocks(body, plane, first, end):
        zz = lax.rem(z + plane, 2)

        def step(yy, carry):
            body(zz, yy)
            return carry

        lax.fori_loop(first, end, step, 0)

    def run(op, *args):
        if op == "s":
            flows[args[0]].stage(args[1])
        elif op == "n1":
            load.wait()
            for copy in small:
                copy.wait()
            over_rows(functools.partial(rms_rows, rows_in, norm_mix, normed))
        elif op == "n2":
            over_rows(functools.partial(rms_rows, rows_in, norm_ffn, normed))
        elif op == "g":
            spatial_group(args[0])
        elif op == "m":
            over_blocks(mix_out, *args)
        elif op == "u":
            gate_up(lax.rem(t + args[0], 2), args[1], args[2])
        else:
            over_blocks(functools.partial(project_down, args[0]), *args[1:])

    for item in SCHEDULE:
        run(*item)
    for flow in flows:
        flow.finish()


def on_device(
    tokens,
    norm_mix,
    w_unit,
    w_value,
    spatial,
    spatial_bias,
    group_gain,
    group_shift,
    w_mix_out,
    norm_ffn,
    w_gate,
    w_up,
    w_down,
):
    count, width = tokens.shape
    half = count // 2
    any_space = pl.BlockSpec(memory_space=pl.ANY)
    vmem = pl.BlockSpec(memory_space=pltpu.VMEM)
    return pl.pallas_call(
        kernel,
        out_shape=pltpu.VMEM((half, width), BF16),
        in_specs=[any_space] * 13,
        out_specs=vmem,
        scratch_shapes=[
            pltpu.VMEM((2, 2, 4, 4, 64, WIDTH), BF16),
            pltpu.VMEM((half, width), BF16),
            pltpu.VMEM((half, width), BF16),
            pltpu.VMEM((half, 512), F32),
            pltpu.VMEM((half, 1024), BF16),
            pltpu.VMEM((half, 2 * HALF_FF), BF16),
            pltpu.VMEM((8, half, 256), F32),
            pltpu.SemaphoreType.DMA((len(FLOWS), 4)),
            pltpu.SemaphoreType.DMA((len(FLOWS), 7)),
            pltpu.VMEM(norm_mix.shape, BF16),
            pltpu.VMEM(spatial.shape, BF16),
            pltpu.VMEM(spatial_bias.shape, BF16),
            pltpu.VMEM(group_gain.shape, BF16),
            pltpu.VMEM(group_shift.shape, BF16),
            pltpu.VMEM(norm_ffn.shape, BF16),
            pltpu.SemaphoreType.DMA((9,)),
        ],
        compiler_params=pltpu.CompilerParams(
            collective_id=0, has_side_effects=True, vmem_limit_bytes=64000000
        ),
    )(
        tokens,
        w_unit,
        w_value,
        w_mix_out.T,
        w_gate,
        w_up,
        w_down.T,
        norm_mix,
        spatial,
        spatial_bias,
        group_gain,
        group_shift,
        norm_ffn,
    )


def solution(mesh):
    placed = (
        P(("rep", "fs"), None),
        P(),
        P("fs", "tp"),
        P("fs", "tp"),
        P(),
        P(),
        P(),
        P(),
        P("tp", "fs"),
        P(),
        P("fs", "tp"),
        P("fs", "tp"),
        P("tp", "fs"),
    )
    return jax.shard_map(
        on_device,
        mesh=mesh,
        in_specs=placed,
        out_specs=P(("rep", "fs", "tp"), None),
        check_vma=False,
    )
```

time: 630 us -> 108 us (0.17)
  waiting for transfers between devices: 467 us -> 0 us
  Pallas kernels: 0 us -> 107 us
  matrix products: 51.8 us -> 0 us
  other arithmetic: 44.6 us -> 0 us
  blocking collectives: 28.2 us -> 0 us
  between operations: 13.3 us -> 0.01 us
  local copies, waits for them, and re-layouts: 14.5 us -> 1.32 us
  starting transfers between devices: 9.5 us -> 0 us
    all_gather x4 -> x0, waiting for transfers between devices: 467 us -> none  [the longest x2 270 us: sent_together(): lax.all_gather(both, axis, axis=dim, tiled=True)]
    pallas_call x0 -> x1, Pallas kernels: none -> 107 us  [on_device(): pl.pallas_call(kernel, out_shape=pltpu.VMEM((half, width), BF16), in_spec...]
    dot_general x5 -> x0, matrix products: 51.8 us -> none  [the longest x1 20.9 us: on_device(): jnp.dot(hidden, down_cols, preferred_element_type=jnp.float32)]
    reduce_sum x6 -> x0, other arithmetic: 39.2 us -> none  [the longest x1 14.4 us: spatial_unit(): spread = jnp.mean(jnp.square(active - center), axis=-1, keepdims=True)]
    all_to_all x1 -> x0, blocking collectives: 28.2 us -> none  [summed_on_arrival(): lax.all_to_all(pieces, axis, split_axis=0, concat_axis=0, tiled=True)]
    all_to_all x1 -> x0, starting transfers between devices: 9.34 us -> none  [sent_to_all(): return lax.all_to_all(copies, axis, split_axis=0, concat_axis=0, tiled=True)]
  transfers between devices with their start and end apart: 5 -> 0, of which waited for: 4 -> 0; matrix products, arithmetic and copies ran while one was open for 11% -> 0% of each run, Pallas kernels for 0% -> 0%
where the time goes in v3:
time: 108 us
  Pallas kernels  107 us (99%)
  local copies, waits for them, and re-layouts  1.32 us (1%)
    pallas_call x1, Pallas kernels, on_device(): pl.pallas_call(kernel, out_shape=pltpu.VMEM((half, width), BF16), in_spec...  107 us

profile of v3, /device:TPU:1, one launch (start us, length us, event | category | flops | bytes accessed | tf_op | source)
XLA Modules:
  0.0 107.9 jit_solution(919614145243584962)
XLA Ops:
  0.0 106.6 %shard_map.127 = bf16[512,2048]{1,0:T(8,128)(2,1)S(1)} custom-call(bf16[1024,2048]{1,0:T(8,128)(2,1)} %tokens.1, bf16[64,512]{1,0:T(8,128)(2,1)} %w_unit.1, bf16[64,512]{1,0:T(8,128)(2,1)} %w_value.1, bf16[64,512]{1,0:T(8,128)(2,1)} %bitcast.3, bf16[64,1408]{1,0:T(8,128)(2,1)} %w_gate.1, bf16[64,1408]{1,0:T(8,128)(2,1)} %w_up.1, bf16[64,1408]{1,0:T(8,128)(2,1)} %bitcast.2, ...), custom_call_target="tpu_custom_call" | custom-call | tf_op jit(solution)/shard_map/pallas_call | solution.py:497
  106.6 1.3 %copy.15 = bf16[512,2048]{1,0:T(8,128)(2,1)} copy(bf16[512,2048]{1,0:T(8,128)(2,1)S(1)} %shard_map.127) | data formatting | bytes 4194304

commit v4 on v3

--- a/solution.py
+++ b/solution.py
@@ -17,20 +17,21 @@
 HALF_FF = 1408
 
 FLOWS = (
-    (0, 2, "yzx"),
-    (2, 2, "yxz"),
-    (4, 1, "yzx"),
+    (0, 2, "yxz"),
+    (2, 2, "xyz"),
+    (4, 1, "yxz"),
     (5, 3, "xyz"),
-    (8, 1, "yxz"),
+    (8, 1, "xyz"),
     (9, 3, "yxz"),
-    (12, 4, "xzy"),
-    (16, 6, "xzy"),
-    (22, 6, "yxz"),
-    (28, 4, "xzy"),
-    (32, 2, "xyz"),
-    (34, 4, "yzx"),
+    (12, 3, "xzy"),
+    (15, 4, "xzy"),
+    (19, 4, "yxz"),
+    (23, 6, "yzx"),
+    (29, 3, "yzx"),
+    (32, 2, "yxz"),
+    (34, 4, "xzy"),
     (38, 4, "yxz"),
-    (42, 3, "yzx"),
+    (42, 3, "xzy"),
 )
 DOWN_PARTS = (
     (0, 512),
@@ -39,136 +40,150 @@
 )
 SCHEDULE = (
     ("s", 3, 0),
+    ("s", 2, 0),
+    ("s", 1, 0),
+    ("s", 9, 0),
+    ("s", 6, 0),
+    ("s", 0, 0),
+    ("n1",),
     ("s", 5, 0),
     ("s", 7, 0),
-    ("s", 1, 0),
-    ("s", 2, 0),
-    ("s", 0, 0),
-    ("n1",),
-    ("s", 6, 0),
+    ("s", 2, 1),
     ("s", 3, 1),
+    ("s", 8, 0),
+    ("s", 12, 0),
+    ("s", 1, 1),
+    ("s", 4, 0),
+    ("s", 9, 1),
+    ("s", 6, 1),
+    ("s", 0, 1),
+    ("s", 7, 1),
     ("s", 5, 1),
-    ("s", 4, 0),
-    ("s", 1, 1),
-    ("s", 2, 1),
-    ("s", 0, 1),
-    ("s", 8, 0),
-    ("s", 7, 1),
+    ("s", 2, 2),
+    ("s", 3, 2),
+    ("s", 8, 1),
+    ("s", 12, 1),
+    ("s", 1, 2),
+    ("s", 4, 1),
+    ("s", 9, 2),
+    ("s", 13, 0),
+    ("s", 0, 2),
+    ("s", 6, 2),
     ("s", 5, 2),
-    ("s", 4, 1),
-    ("s", 1, 2),
-    ("s", 2, 2),
-    ("s", 6, 1),
-    ("s", 10, 0),
-    ("s", 3, 2),
-    ("s", 0, 2),
     ("s", 7, 2),
     ("s", 2, 3),
-    ("s", 8, 1),
+    ("s", 12, 2),
     ("s", 4, 2),
-    ("s", 0, 3),
-    ("s", 5, 3),
-    ("s", 9, 0),
-    ("s", 11, 0),
-    ("s", 12, 0),
+    ("s", 10, 0),
     ("s", 3, 3),
     ("s", 8, 2),
+    ("s", 0, 3),
+    ("s", 11, 0),
+    ("s", 9, 3),
+    ("s", 1, 3),
+    ("s", 6, 3),
+    ("s", 13, 1),
+    ("s", 5, 3),
+    ("s", 2, 4),
+    ("s", 14, 0),
+    ("s", 4, 3),
     ("s", 7, 3),
-    ("s", 1, 3),
-    ("s", 6, 2),
+    ("s", 10, 1),
+    ("s", 12, 3),
+    ("s", 3, 4),
     ("s", 11, 1),
-    ("s", 10, 1),
-    ("s", 13, 0),
-    ("s", 12, 1),
-    ("s", 2, 4),
-    ("s", 3, 4),
-    ("s", 6, 3),
-    ("s", 4, 3),
+    ("s", 1, 4),
+    ("s", 8, 3),
+    ("s", 2, 5),
+    ("s", 2, 6),
     ("s", 0, 4),
-    ("s", 5, 4),
+    ("s", 2, 7),
+    ("s", 6, 4),
     ("s", 3, 5),
     ("s", 3, 6),
-    ("s", 9, 1),
+    ("s", 13, 2),
+    ("s", 4, 4),
     ("s", 3, 7),
+    ("g", 1),
+    ("s", 1, 5),
+    ("s", 1, 6),
+    ("g", 3),
+    ("s", 9, 4),
+    ("s", 1, 7),
+    ("s", 0, 5),
+    ("s", 0, 6),
+    ("s", 5, 4),
     ("s", 7, 4),
-    ("s", 11, 2),
-    ("s", 13, 1),
-    ("s", 8, 3),
+    ("s", 14, 1),
+    ("s", 10, 2),
+    ("s", 4, 5),
+    ("s", 4, 6),
+    ("s", 8, 4),
+    ("s", 0, 7),
+    ("g", 0),
+    ("g", 2),
     ("s", 5, 5),
     ("s", 5, 6),
-    ("s", 12, 2),
-    ("s", 1, 4),
-    ("s", 10, 2),
-    ("s", 2, 5),
-    ("s", 11, 3),
-    ("s", 4, 4),
+    ("s", 4, 7),
+    ("s", 13, 3),
+    ("m", 0, 0, 2),
+    ("s", 12, 4),
+    ("s", 11, 2),
+    ("m", 0, 2, 4),
+    ("s", 10, 3),
     ("s", 5, 7),
-    ("s", 2, 7),
-    ("g", 1),
-    ("s", 9, 2),
-    ("s", 1, 5),
-    ("s", 1, 6),
-    ("s", 0, 5),
-    ("g", 3),
-    ("s", 6, 4),
-    ("s", 1, 7),
-    ("s", 4, 5),
-    ("s", 8, 4),
-    ("s", 4, 6),
-    ("s", 0, 7),
-    ("g", 0),
-    ("s", 9, 3),
-    ("g", 2),
-    ("s", 12, 3),
-    ("s", 4, 7),
-    ("m", 0, 0, 4),
+    ("m", 1, 0, 4),
+    ("s", 6, 5),
+    ("n2",),
+    ("s", 9, 5),
+    ("u", 0, 6, 2),
+    ("s", 6, 7),
+    ("s", 14, 2),
+    ("s", 13, 4),
+    ("s", 9, 7),
+    ("u", 1, 6, 2),
     ("s", 7, 5),
-    ("m", 1, 0, 2),
-    ("s", 13, 2),
-    ("m", 1, 2, 4),
-    ("n2",),
-    ("s", 10, 3),
-    ("s", 7, 7),
-    ("u", 0, 2, 2),
-    ("u", 1, 2, 2),
-    ("s", 11, 4),
-    ("s", 6, 5),
     ("u", 0, 0, 2),
-    ("s", 12, 4),
     ("s", 8, 5),
     ("s", 8, 6),
+    ("s", 11, 3),
+    ("u", 0, 2, 2),
+    ("s", 7, 7),
+    ("s", 14, 3),
+    ("u", 1, 0, 2),
+    ("s", 12, 5),
     ("u", 0, 4, 2),
-    ("u", 0, 6, 2),
-    ("s", 6, 7),
-    ("s", 13, 3),
-    ("u", 1, 0, 2),
+    ("s", 8, 7),
+    ("u", 1, 2, 2),
+    ("s", 12, 7),
+    ("d", 0, 0, 0, 2),
+    ("s", 10, 4),
+    ("d", 0, 0, 2, 4),
+    ("s", 11, 4),
+    ("u", 1, 4, 2),
+    ("d", 0, 1, 0, 4),
+    ("s", 13, 5),
+    ("s", 14, 4),
+    ("s", 13, 6),
+    ("d", 1, 0, 0, 4),
+    ("s", 10, 5),
+    ("u", 0, 8, 2),
+    ("s", 13, 7),
+    ("d", 1, 1, 2, 4),
+    ("d", 1, 1, 0, 2),
     ("s", 11, 5),
-    ("s", 8, 7),
-    ("u", 1, 4, 2),
-    ("s", 9, 4),
-    ("u", 1, 6, 2),
-    ("s", 10, 4),
+    ("s", 11, 6),
+    ("u", 0, 10, 1),
+    ("s", 10, 7),
+    ("s", 14, 5),
+    ("u", 1, 8, 2),
     ("s", 11, 7),
-    ("d", 0, 0, 0, 4),
-    ("d", 0, 1, 0, 2),
-    ("s", 12, 5),
-    ("s", 12, 6),
-    ("s", 13, 4),
-    ("d", 0, 1, 2, 4),
-    ("d", 1, 0, 0, 4),
-    ("s", 9, 5),
-    ("s", 12, 7),
-    ("d", 1, 1, 0, 4),
-    ("s", 10, 5),
-    ("s", 10, 6),
-    ("u", 0, 8, 3),
-    ("s", 9, 7),
-    ("s", 13, 5),
-    ("s", 10, 7),
-    ("u", 1, 8, 3),
-    ("s", 13, 7),
-    ("d", 2, 0, 0, 4),
-    ("d", 2, 1, 0, 4),
+    ("u", 1, 10, 1),
+    ("s", 14, 7),
+    ("d", 2, 1, 2, 4),
+    ("d", 2, 0, 0, 2),
+    ("d", 2, 1, 0, 2),
+    ("d", 2, 0, 2, 4),
 )
 class Flow:
     def __init__(self, index, buf, send_sems, recv_sems, where):
@@ -375,11 +390,8 @@
     blocks = count // LANES
 
     def over_rows(body):
-        def step(i, carry):
-            body(pl.ds(pl.multiple_of(i * LANES, LANES), LANES))
-            return carry
-
-        lax.fori_loop(0, blocks, step, 0)
+        for i in range(blocks):
+            body(pl.ds(i * LANES, LANES))
 
     def columns(tt, first, size):
         return buf[tt, :, :, :, :, pl.ds(first, size)].reshape(2048, size)
@@ -417,15 +429,11 @@
         rows_in[:, cols] = total.astype(BF16)
 
     def gate_up(tt, pair, pairs):
-        def step(i, carry):
-            first = pl.multiple_of(PAIRS + i * 256, 256)
-            both = dot(normed[...], columns(tt, first, 256))
+        for i in range(pair, pair + pairs):
+            both = dot(normed[...], columns(tt, PAIRS + i * 256, 256))
             value = jax.nn.silu(both[:, 0:128]) * both[:, 128:256]
             into = pl.ds(pl.multiple_of(tt * HALF_FF + i * 128, 128), 128)
             hidden[:, into] = value.astype(BF16)
-            return carry
-
-        lax.fori_loop(pair, pair + pairs, step, 0)
 
     def project_down(part, zz, yy):
         first, size = DOWN_PARTS[part]
@@ -444,11 +452,8 @@
     def over_blocks(body, plane, first, end):
         zz = lax.rem(z + plane, 2)
 
-        def step(yy, carry):
+        for yy in range(first, end):
             body(zz, yy)
-            return carry
-
-        lax.fori_loop(first, end, step, 0)
 
     def run(op, *args):
         if op == "s":

time: 108 us -> 106 us (0.981)
  Pallas kernels: 107 us -> 104 us
    pallas_call x1, Pallas kernels: 107 us -> 104 us  [on_device(): pl.pallas_call(kernel, out_shape=pltpu.VMEM((half, width), BF16), in_spec...]
where the time goes in v4:
time: 106 us
  Pallas kernels  104 us (98%)
  local copies, waits for them, and re-layouts  1.32 us (1%)
    pallas_call x1, Pallas kernels, on_device(): pl.pallas_call(kernel, out_shape=pltpu.VMEM((half, width), BF16), in_spec...  104 us

profile of v4, /device:TPU:1, one launch (start us, length us, event | category | flops | bytes accessed | tf_op | source)
XLA Modules:
  0.0 105.6 jit_solution(112204788724024879)
XLA Ops:
  0.0 104.2 %shard_map.127 = bf16[512,2048]{1,0:T(8,128)(2,1)S(1)} custom-call(bf16[1024,2048]{1,0:T(8,128)(2,1)} %tokens.1, bf16[64,512]{1,0:T(8,128)(2,1)} %w_unit.1, bf16[64,512]{1,0:T(8,128)(2,1)} %w_value.1, bf16[64,512]{1,0:T(8,128)(2,1)} %bitcast.3, bf16[64,1408]{1,0:T(8,128)(2,1)} %w_gate.1, bf16[64,1408]{1,0:T(8,128)(2,1)} %w_up.1, bf16[64,1408]{1,0:T(8,128)(2,1)} %bitcast.2, ...), custom_call_target="tpu_custom_call" | custom-call | tf_op jit(solution)/shard_map/pallas_call | solution.py:502
  104.3 1.3 %copy.15 = bf16[512,2048]{1,0:T(8,128)(2,1)} copy(bf16[512,2048]{1,0:T(8,128)(2,1)S(1)} %shard_map.127) | data formatting | bytes 4194304
